TPU v7x, 32 devices: a whole 2x2x4 slice. The times are simulated.
32 devices in a mesh: sp: 8 (over z, y), tp: 4 (over x, core).
Axes of the slice: x: 2, y: 2, z: 4, core: 2. Of those that a mesh axis runs over, the one named last changes fastest.
Arguments:
- inputs: bfloat16 [2, 3072, 4096], P(None, 'sp'), may hold values from -8 to 8
- w_key: bfloat16 [4096, 2048], P(None, 'tp'), may hold values from -0.09375 to 0.09375
- w_value: bfloat16 [4096, 2048], P(None, 'tp'), may hold values from -0.09375 to 0.09375
- w_query: bfloat16 [4096, 2048], P(None, 'tp'), may hold values from -0.09375 to 0.09375
- w_igate: bfloat16 [4096, 16], replicated, may hold values from -1 to 1
- w_fgate: bfloat16 [4096, 16], replicated, may hold values from -0.09375 to 0.09375
- forget_bias: float32 [16], replicated, may hold values from 3 to 12
- new_rows: bfloat16 [2, 4096], P(None, 'tp'), may hold values from -6 to 6
Outputs:
- cache_matrix: bfloat16 [2, 16, 128, 128], P(None, 'tp', 'sp')
- cache_normal: float32 [2, 16, 128], P(None, 'tp', 'sp')
- cache_top: float32 [2, 16], P(None, 'tp')
- read: bfloat16 [2, 16, 128], P(None, 'tp', 'sp')
All inputs are finite; a program needn't handle non-finite values.
Results may differ from a plain program's by a relative error of at most 0.015.
Values may be sent and summed in bfloat16 or wider, within the bound.
A program may use at most 64 MiB of HBM per device.

v0:
```python
import jax
import jax.numpy as jnp
from jax import lax
from jax.sharding import PartitionSpec as P

DH = 128
EPS = 1e-06


def prefix(value, axis, combine, identity):
    devices, here = (lax.axis_size(axis), lax.axis_index(axis))
    everything = lax.all_gather(value, axis)
    start = jnp.broadcast_to(jnp.asarray(identity, value.dtype), value.shape)

    def lap(k, before):
        at = devices - 1 - k
        reached = at > here
        new = combine(before, everything[at])
        return jnp.where(reached, new, before)

    return lax.fori_loop(0, devices, lap, start)


def normalize(row_block):
    scaled = row_block.astype(jnp.float32)
    scaled = scaled * lax.rsqrt(jnp.mean(scaled * scaled, axis=-1, keepdims=True) + EPS)
    return scaled.astype(jnp.bfloat16)


def add_pair(earlier, second):
    return earlier + second


def shards(inputs, w_key, w_value, w_query, w_igate, w_fgate, forget_bias, new_rows):
    head_count = w_key.shape[1] // DH
    seq_count, span, width = inputs.shape
    rows_own = DH // lax.axis_size("sp")
    row_start = lax.axis_index("sp") * rows_own
    head_start = lax.axis_index("tp") * head_count
    gate_in = lax.dynamic_slice_in_dim(w_igate, head_start, head_count, 1)
    gate_forget = lax.dynamic_slice_in_dim(w_fgate, head_start, head_count, 1)
    bias_heads = lax.dynamic_slice_in_dim(forget_bias, head_start, head_count, 0)
    normed = normalize(inputs)
    key_rows = jnp.einsum("spd,dc->spc", normed, w_key, preferred_element_type=jnp.float32).astype(
        jnp.bfloat16
    )
    value_rows = jnp.einsum(
        "spd,dc->spc", normed, w_value, preferred_element_type=jnp.float32
    ).astype(jnp.bfloat16)
    input_pre = jnp.einsum("spd,dh->sph", normed, gate_in, preferred_element_type=jnp.float32)
    log_forget = jax.nn.log_sigmoid(
        jnp.einsum("spd,dh->sph", normed, gate_forget, preferred_element_type=jnp.float32)
        + bias_heads
    )
    running = jnp.cumsum(log_forget, axis=1)
    own_total = running[:, -1, :]
    beyond = prefix(own_total, "sp", add_pair, jnp.zeros_like(own_total))
    log_weight = (beyond + own_total)[:, None, :] - running + input_pre
    stabilizer = lax.pmax(jnp.max(log_weight, axis=1), "sp")
    weight = jnp.exp(log_weight - stabilizer[:, None, :])
    key_heads = key_rows.reshape(seq_count, span, head_count, DH)
    value_heads = value_rows.reshape(seq_count, span, head_count, DH)
    weighted = (weight[..., None] * value_heads.astype(jnp.float32)).astype(jnp.bfloat16)
    partial_normal = jnp.einsum("sth,sthd->shd", weight, key_heads.astype(jnp.float32))
    partial_matrix = jnp.einsum(
        "sthe,sthd->shed", weighted, key_heads, preferred_element_type=jnp.float32
    )
    matrix, normal = (
        lax.psum_scatter(partial_matrix, "sp", scatter_dimension=2, tiled=True),
        lax.psum_scatter(partial_normal, "sp", scatter_dimension=2, tiled=True),
    )
    cache_matrix = matrix.astype(jnp.bfloat16)
    new_normed = normalize(lax.all_gather(new_rows, "tp", axis=1, tiled=True))
    query_new = jnp.dot(new_normed, w_query, preferred_element_type=jnp.float32).astype(
        jnp.bfloat16
    )
    key_new = jnp.dot(new_normed, w_key, preferred_element_type=jnp.float32).astype(jnp.bfloat16)
    value_new = jnp.dot(new_normed, w_value, preferred_element_type=jnp.float32).astype(
        jnp.bfloat16
    )
    query_new = query_new.astype(jnp.float32).reshape(seq_count, head_count, DH)
    key_new = key_new.astype(jnp.float32).reshape(seq_count, head_count, DH)
    value_new = value_new.astype(jnp.float32).reshape(seq_count, head_count, DH)
    value_own = lax.dynamic_slice_in_dim(value_new, row_start, rows_own, 2)
    query_own = lax.dynamic_slice_in_dim(query_new, row_start, rows_own, 2)
    input_new = jnp.dot(new_normed, gate_in, preferred_element_type=jnp.float32)
    forget_new = jax.nn.log_sigmoid(
        jnp.dot(new_normed, gate_forget, preferred_element_type=jnp.float32) + bias_heads
    )
    top_next = jnp.maximum(forget_new + stabilizer, input_new)
    old_share = jnp.exp(forget_new + stabilizer - top_next)
    new_share = jnp.exp(input_new - top_next)
    agreement = jnp.sum(key_new * query_new, axis=-1)
    factor = DH ** (-0.5)
    numerator = old_share[..., None] * jnp.einsum(
        "shed,shd->she", cache_matrix.astype(jnp.float32), query_new
    )
    numerator = (numerator + (new_share * agreement)[..., None] * value_own) * factor
    normal_dot = lax.psum(jnp.sum(normal * query_own, axis=-1), "sp")
    denominator = (old_share * normal_dot + new_share * agreement) * factor
    read = numerator / jnp.maximum(jnp.abs(denominator), 1.0)[..., None]
    return (cache_matrix, normal, stabilizer, read.astype(jnp.bfloat16))


def solution(mesh):
    in_specs = (
        P(None, "sp", None),
        P(None, "tp"),
        P(None, "tp"),
        P(None, "tp"),
        P(),
        P(),
        P(),
        P(None, "tp"),
    )
    out_specs = (P(None, "tp", "sp", None), P(None, "tp", "sp"), P(None, "tp"), P(None, "tp", "sp"))
    return jax.shard_map(shards, mesh=mesh, in_specs=in_specs, out_specs=out_specs, check_vma=False)
```

profile of v0, /device:TPU:0, one launch (start us, length us, event | category | flops | bytes accessed | tf_op | source)
XLA Modules:
  0.0 208.2 jit_solution(13657243341448075160)
XLA Ops:
  7.2 0.0 copy-start
  7.2 0.0 copy-start.7
  7.2 0.0 reduce-scatter.7.cloned.1.call-start
  7.2 0.0 copy-start.6
  7.3 4.1 %fusion = f32[2,384]{1,0:T(2,128)S(1)} fusion(bf16[2,384,4096]{2,1,0:T(8,128)(2,1)} %param.10), kind=kLoop, calls=%fused_computation.3 | loop fusion | flops 9436416 | bytes 6294528 | tf_op jit(solution)/shard_map/reduce_sum | solution.py:26
  11.4 0.0 copy-done.7
  11.4 0.1 dynamic_slice.26
  11.5 0.0 copy-done
  11.5 4.6 %fusion.64 = f32[2,4,3,128]{3,1,2,0:T(4,128)S(1)} fusion(bf16[4096,16]{0,1:T(8,128)(2,1)S(1)} %copy-done, s32[]{:T(128)S(6)} %select_n.52, bf16[2,384,4096]{2,1,0:T(8,128)(2,1)} %param.10, f32[2,384]{1,0:T(2,128)S(1)} %add_rsqrt_fusion, f32[4]{0:T(128)S(1)} %dynamic_slice.26), kind=kOutput, calls=%fused_computation.47 | convolution fusion | flops 34630656 | bytes 6340100 | tf_op jit(solution)/shard_map/spd,dh->sph/dot_general | solution.py:52
  16.1 2.4 %reduce-window.6 = f32[2,4,3,128]{3,2,1,0:T(4,128)S(1)} reduce-window(f32[2,4,3,128]{3,2,1,0:T(4,128)S(1)} %copy.21, f32[]{:T(128)} %constant.74.clone.1), window={size=1x1x1x128 pad=0_0x0_0x0_0x127_0}, to_apply=%region_1.2 | reduce-window | flops 390144 | bytes 24580 | tf_op jit(solution)/shard_map/reduce-window
  18.5 0.1 slice.12
  18.6 0.1 copy.22
  18.8 0.1 copy.23
  18.9 0.1 broadcast_add_fusion
  19.0 0.2 slice_reduce_fusion
  19.1 0.1 copy.24
  19.2 22.3 %all-gather = f32[16,1,4]{2,1,0:T(1,128)S(1)} all-gather(f32[2,1,4]{2,1,0:T(1,128)S(1)} %copy.24), channel_id=2, replica_groups=mesh['sp'=8,'tp'=4] {'sp'}, dimensions={0}, use_global_device_ids=true | all-gather | bytes 288 | tf_op jit(solution)/shard_map/all_gather | solution.py:12
  41.5 0.3 while.16
  41.8 0.0 copy-done.6
  41.8 4.7 %fusion.91 = (f32[2,4]{1,0:T(2,128)S(1)}, f32[2,384,4]{1,2,0:T(4,128)S(1)}) fusion(bf16[4096,16]{0,1:T(8,128)(2,1)S(1)} %copy-done.6, s32[]{:T(128)S(6)} %select_n.52, bf16[2,384,4096]{2,1,0:T(8,128)(2,1)} %param.10, f32[2,384]{1,0:T(2,128)S(1)} %add_rsqrt_fusion, f32[2,4,384]{2,1,0:T(4,128)S(1)} %reduce_window_sum.16, f32[2,4]{1,0:T(2,128)S(1)} %add.125), kind=kOutput, calls=%fused_computation.73 | convolution fusion | flops 34612216 | bytes 6352932 | tf_op jit(solution)/shard_map/spd,dh->sph/dot_general | solution.py:50
  46.5 17.1 %pmax.7 = f32[2,4]{1,0:T(2,128)S(1)} all-reduce(f32[2,4]{1,0:T(2,128)S(1)} %get-tuple-element.143), channel_id=1, replica_groups=mesh['sp'=8,'tp'=4] {'sp'}, use_global_device_ids=true, to_apply=%region_6.7 | all-reduce | flops 8 | bytes 64 | tf_op jit(solution)/shard_map/pmax | solution.py:59
  63.6 0.0 copy-start.4
  63.6 7.5 %fusion.27 = bf16[2,48,4,8,128]{4,3,2,1,0:T(8,128)(2,1)S(1)} fusion(bf16[4096,512]{1,0:T(8,128)(2,1)} %param.11, bf16[2,384,4096]{2,1,0:T(8,128)(2,1)} %param.10, f32[2,384]{1,0:T(2,128)S(1)} %add_rsqrt_fusion), kind=kOutput, calls=%fused_computation.15 | convolution fusion | flops 3231055872 | bytes 11275264 | tf_op jit(solution)/shard_map/spd,dc->spc/dot_general | solution.py:44
  71.1 0.0 copy-start.1
  71.1 0.1 fusion.98
  71.2 0.8 copy-done.1
  72.0 0.2 fusion.48
  72.2 0.2 copy.32
  72.4 0.7 reshape.91
  73.1 0.0 reduce-scatter.7.cloned.1.call-update
  73.2 0.0 reduce-scatter.5.cloned.1.call-start
  73.2 0.1 subtract_exponential_fusion
  73.3 6.9 %fusion.17 = f32[2,384,512]{2,1,0:T(8,128)S(1)} fusion(bf16[4096,512]{1,0:T(8,128)(2,1)} %param.12, bf16[2,384,4096]{2,1,0:T(8,128)(2,1)} %param.10, f32[2,384]{1,0:T(2,128)S(1)} %add_rsqrt_fusion), kind=kOutput, calls=%fused_computation.13 | convolution fusion | flops 3231449088 | bytes 12061696 | tf_op jit(solution)/shard_map/spd,dc->spc/dot_general | solution.py:47
  80.2 0.0 copy-start.5
  80.2 0.5 copy.31
  80.7 2.3 %fusion.47 = f32[2,4,128,128]{3,2,1,0:T(8,128)} fusion(f32[2,384,4,128]{1,3,2,0:T(8,128)S(1)} %bitcast.61, f32[2,384,4]{1,2,0:T(4,128)S(1)} %subtract_exponential_fusion, bf16[2,48,4,8,128]{4,3,2,1,0:T(8,128)(2,1)} %copy-done.1), kind=kOutput, calls=%fused_computation.27 | convolution fusion | flops 101449728 | bytes 2895872 | tf_op jit(solution)/shard_map/sthe,sthd->shed/dot_general | solution.py:65
  83.0 0.0 reduce-scatter.5.cloned.1.call-update
  83.0 0.0 copy-done.5
  83.0 5.2 %all_gather.7 = bf16[2,4096]{1,0:T(2,128)(2,1)S(1)} all-gather(bf16[2,1024]{1,0:T(2,128)(2,1)S(1)} %copy-done.5), channel_id=1, replica_groups=mesh['sp'=8,'tp'=4] {'tp'}, dimensions={1}, use_global_device_ids=true | all-gather | bytes 20480 | tf_op jit(solution)/shard_map/all_gather | solution.py:73
  88.2 0.1 fusion.54
  88.4 2.9 %fusion.45 = f32[2,512]{1,0:T(2,128)S(1)} fusion(bf16[4096,512]{1,0:T(8,128)(2,1)} %param.11, bf16[2,4096]{1,0:T(2,128)(2,1)S(1)} %all_gather.7, f32[2]{0:T(128)S(1)} %add_rsqrt_fusion.1), kind=kOutput, calls=%fused_computation.23 | convolution fusion | flops 8415232 | bytes 4214792 | tf_op jit(solution)/shard_map/dot_general | solution.py:77
  91.3 2.9 %convolution_convert_fusion.2 = bf16[2,512]{1,0:T(2,128)(2,1)S(1)} fusion(bf16[4096,512]{1,0:T(8,128)(2,1)} %param.13, bf16[2,4096]{1,0:T(2,128)(2,1)S(1)} %all_gather.7, f32[2]{0:T(128)S(1)} %add_rsqrt_fusion.1), kind=kOutput, calls=%fused_computation.24 | convolution fusion | flops 8414208 | bytes 4212744 | tf_op jit(solution)/shard_map/dot_general | solution.py:74
  94.2 0.1 multiply_reduce_fusion.1
  94.3 0.2 fusion.58
  94.5 2.9 %fusion.44 = f32[2,512]{1,0:T(2,128)S(1)} fusion(bf16[4096,512]{1,0:T(8,128)(2,1)} %param.12, bf16[2,4096]{1,0:T(2,128)(2,1)S(1)} %all_gather.7, f32[2]{0:T(128)S(1)} %add_rsqrt_fusion.1), kind=kOutput, calls=%fused_computation.21 | convolution fusion | flops 8415232 | bytes 4214792 | tf_op jit(solution)/shard_map/dot_general | solution.py:78
  97.4 37.1 %reduce-scatter.7.cloned.1.call-done = f32[16,8]{1,0:T(8,128)} async-done(((f32[128,8]{1,0:T(8,128)}), f32[16,8]{1,0:T(8,128)}) %reduce-scatter.7.cloned.1.call-update) | async-done | bytes 528
  134.6 0.8 reshape.92
  135.3 0.1 copy.33
  135.4 0.0 copy-start.3
  135.4 0.2 multiply_reduce_fusion
  135.6 19.5 %psum.7 = f32[2,4]{1,0:T(2,128)S(1)} all-reduce(f32[2,4]{1,0:T(2,128)S(1)} %multiply_reduce_fusion), channel_id=1, replica_groups=mesh['sp'=8,'tp'=4] {'sp'}, use_global_device_ids=true, to_apply=%region_12.13 | all-reduce | flops 8 | bytes 64 | tf_op jit(solution)/shard_map/psum | solution.py:99
  155.1 0.0 copy-done.4
  155.1 0.2 abs_maximum_fusion
  155.4 44.3 %reduce-scatter.5.cloned.1.call-done = f32[2,4,16,128]{3,2,1,0:T(8,128)} async-done(((f32[2,4,128,128]{3,2,1,0:T(8,128)}), f32[2,4,16,128]{3,2,1,0:T(8,128)}) %reduce-scatter.5.cloned.1.call-update) | async-done | bytes 65552 | tf_op jit(solution)/shard_map/reduce_scatter | solution.py:69
  199.7 0.8 convert_element_type.54
  200.5 0.0 copy-start.2
  200.5 0.1 fusion.92
  200.6 0.7 fusion.70
  201.3 0.0 copy-done.3
  201.3 0.0 copy-done.2
  (21 shorter events, 0.2 us)
Async XLA Ops:
  7.2 4.3 %copy-start = (bf16[4096,16]{0,1:T(8,128)(2,1)S(1)}, bf16[4096,16]{0,1:T(8,128)(2,1)}, u32[]{:S(2)}) copy-start(bf16[4096,16]{0,1:T(8,128)(2,1)} %param.15) | copy-start | bytes 393220
  7.2 4.2 %copy-start.7 = (f32[16]{0:T(128)S(1)}, f32[16]{0:T(128)}, u32[]{:S(2)}) copy-start(f32[16]{0:T(128)} %param.16) | copy-start | bytes 196
  7.2 127.4 %reduce-scatter.7.cloned.1.call-start = ((), (), s32[]{:S(2)}) async-start(), calls=%async_computation.3 | async-start | bytes 73728
  7.2 34.6 %copy-start.6 = (bf16[4096,16]{0,1:T(8,128)(2,1)S(1)}, bf16[4096,16]{0,1:T(8,128)(2,1)}, u32[]{:S(2)}) copy-start(bf16[4096,16]{0,1:T(8,128)(2,1)} %param.14) | copy-start | bytes 393220
  63.6 91.5 %copy-start.4 = (f32[2,4]{1,0:T(2,128)}, f32[2,4]{1,0:T(2,128)S(1)}, u32[]{:S(2)}) copy-start(f32[2,4]{1,0:T(2,128)S(1)} %pmax.7) | copy-start | bytes 100
  71.1 0.9 copy-start.1
  73.2 126.5 %reduce-scatter.5.cloned.1.call-start = ((), (), s32[]{:S(2)}) async-start(), calls=%async_computation.2 | async-start | bytes 589824 | tf_op jit(solution)/shard_map/reduce_scatter | solution.py:69
  80.2 2.8 %copy-start.5 = (bf16[2,1024]{1,0:T(2,128)(2,1)S(1)}, bf16[2,1024]{1,0:T(2,128)(2,1)}, u32[]{:S(2)}) copy-start(bf16[2,1024]{1,0:T(2,128)(2,1)} %param.17) | copy-start | bytes 12292
  135.4 65.9 %copy-start.3 = (f32[2,4,16]{2,1,0:T(4,128)}, f32[2,4,16]{2,1,0:T(4,128)S(1)}, u32[]{:S(2)}) copy-start(f32[2,4,16]{2,1,0:T(4,128)S(1)} %copy.33) | copy-start | bytes 1540
  200.5 0.8 copy-start.2
Sparse Core Ops, SparseCore 0:
  73.3 61.2 reduce-scatter.6
  137.9 61.7 reduce-scatter.4
where the time goes:
time: 209 us; the launch traced here: 208 us
  waiting for transfers between devices  81.5 us (39%)
  blocking collectives  64.1 us (31%)
  matrix products  35.4 us (17%)
  between operations  14.2 us (7%)
  other arithmetic  8.84 us (4%)
  local copies, waits for them, and re-layouts  3.79 us (2%)
    reduce_scatter x1, waiting for transfers between devices, shards(): lax.psum_scatter(partial_matrix, 'sp', scatter_dimension=2, tiled=True)  44.3 us
    unnamed x3, waiting for transfers between devices  37.2 us
    all_gather x1, blocking collectives, prefix(): everything = lax.all_gather(value, axis)  22.3 us
    psum x1, blocking collectives, shards(): normal_dot = lax.psum(jnp.sum(normal * query_own, axis=-1), 'sp')  19.5 us
    pmax x1, blocking collectives, shards(): stabilizer = lax.pmax(jnp.max(log_weight, axis=1), 'sp')  17.1 us
    dot_general x1, matrix products, shards(): jnp.einsum('spd,dc->spc', normed, w_key, preferred_element_type=jnp.float32)  7.46 us
    dot_general x1, matrix products, shards(): jnp.einsum('spd,dc->spc', normed, w_value, preferred_element_type=jnp.flo...  6.89 us
    all_gather x1, blocking collectives, shards(): new_normed = normalize(lax.all_gather(new_rows, 'tp', axis=1, tiled=True))  5.21 us
  transfers between devices with their start and end apart: 2, of which 2 were waited for; matrix products, arithmetic and copies ran while one was open for 10% of the time, Pallas kernels for 0%

commit v1 on v0

--- a/solution.py
+++ b/solution.py
@@ -96,7 +96,9 @@
         "shed,shd->she", cache_matrix.astype(jnp.float32), query_new
     )
     numerator = (numerator + (new_share * agreement)[..., None] * value_own) * factor
-    normal_dot = lax.psum(jnp.sum(normal * query_own, axis=-1), "sp")
+    part = jnp.sum(normal * query_own, axis=-1)
+    shards_2 = lax.all_gather(part, "sp")
+    normal_dot = jnp.sum(shards_2, axis=0)
     denominator = (old_share * normal_dot + new_share * agreement) * factor
     read = numerator / jnp.maximum(jnp.abs(denominator), 1.0)[..., None]
     return (cache_matrix, normal, stabilizer, read.astype(jnp.bfloat16))

time: 209 us -> 209 us (level)
    psum x1 -> x0, blocking collectives: 19.5 us -> none  [shards(): normal_dot = lax.psum(jnp.sum(normal * query_own, axis=-1), 'sp')]
    all_gather x0 -> x1, blocking collectives: none -> 18.6 us  [shards(): shards_2 = lax.all_gather(part, 'sp')]
where the time goes in v1:
time: 209 us; the launch traced here: 208 us
  waiting for transfers between devices  82.3 us (39%)
  blocking collectives  63.3 us (30%)
  matrix products  35.4 us (17%)
  between operations  14.2 us (7%)
  other arithmetic  8.86 us (4%)
  local copies, waits for them, and re-layouts  3.79 us (2%)
    reduce_scatter x1, waiting for transfers between devices, shards(): lax.psum_scatter(partial_matrix, 'sp', scatter_dimension=2, tiled=True)  45.2 us
    unnamed x3, waiting for transfers between devices  37.2 us
    all_gather x1, blocking collectives, prefix(): everything = lax.all_gather(value, axis)  22.3 us
    all_gather x1, blocking collectives, shards(): shards_2 = lax.all_gather(part, 'sp')  18.6 us
    pmax x1, blocking collectives, shards(): stabilizer = lax.pmax(jnp.max(log_weight, axis=1), 'sp')  17.1 us
    dot_general x1, matrix products, shards(): jnp.einsum('spd,dc->spc', normed, w_key, preferred_element_type=jnp.float32)  7.46 us
    dot_general x1, matrix products, shards(): jnp.einsum('spd,dc->spc', normed, w_value, preferred_element_type=jnp.flo...  6.89 us
    all_gather x1, blocking collectives, shards(): new_normed = normalize(lax.all_gather(new_rows, 'tp', axis=1, tiled=True))  5.21 us
  transfers between devices with their start and end apart: 2, of which 2 were waited for; matrix products, arithmetic and copies ran while one was open for 10% of the time, Pallas kernels for 0%

profile of v1, /device:TPU:0, one launch (start us, length us, event | category | flops | bytes accessed | tf_op | source)
XLA Modules:
  0.0 208.1 jit_solution(15284433392969613356)
XLA Ops:
  7.2 0.0 copy-start
  7.2 0.0 copy-start.7
  7.2 0.0 reduce-scatter.7.cloned.1.call-start
  7.2 0.0 copy-start.6
  7.3 4.1 %fusion = f32[2,384]{1,0:T(2,128)S(1)} fusion(bf16[2,384,4096]{2,1,0:T(8,128)(2,1)} %param.10), kind=kLoop, calls=%fused_computation.3 | loop fusion | flops 9436416 | bytes 6294528 | tf_op jit(solution)/shard_map/reduce_sum | solution.py:26
  11.4 0.0 copy-done.7
  11.4 0.1 dynamic_slice.26
  11.5 0.0 copy-done
  11.5 4.6 %fusion.64 = f32[2,4,3,128]{3,1,2,0:T(4,128)S(1)} fusion(bf16[4096,16]{0,1:T(8,128)(2,1)S(1)} %copy-done, s32[]{:T(128)S(6)} %select_n.52, bf16[2,384,4096]{2,1,0:T(8,128)(2,1)} %param.10, f32[2,384]{1,0:T(2,128)S(1)} %add_rsqrt_fusion, f32[4]{0:T(128)S(1)} %dynamic_slice.26), kind=kOutput, calls=%fused_computation.47 | convolution fusion | flops 34630656 | bytes 6340100 | tf_op jit(solution)/shard_map/spd,dh->sph/dot_general | solution.py:52
  16.1 2.4 %reduce-window.6 = f32[2,4,3,128]{3,2,1,0:T(4,128)S(1)} reduce-window(f32[2,4,3,128]{3,2,1,0:T(4,128)S(1)} %copy.21, f32[]{:T(128)} %constant.74.clone.1), window={size=1x1x1x128 pad=0_0x0_0x0_0x127_0}, to_apply=%region_1.2 | reduce-window | flops 390144 | bytes 24580 | tf_op jit(solution)/shard_map/reduce-window
  18.5 0.1 slice.12
  18.6 0.1 copy.22
  18.8 0.1 copy.23
  18.9 0.1 broadcast_add_fusion
  19.0 0.2 slice_reduce_fusion
  19.1 0.1 copy.24
  19.2 22.3 %all-gather = f32[16,1,4]{2,1,0:T(1,128)S(1)} all-gather(f32[2,1,4]{2,1,0:T(1,128)S(1)} %copy.24), channel_id=2, replica_groups=mesh['sp'=8,'tp'=4] {'sp'}, dimensions={0}, use_global_device_ids=true | all-gather | bytes 288 | tf_op jit(solution)/shard_map/all_gather | solution.py:12
  41.5 0.3 while.16
  41.8 0.0 copy-done.6
  41.8 4.7 %fusion.91 = (f32[2,4]{1,0:T(2,128)S(1)}, f32[2,384,4]{1,2,0:T(4,128)S(1)}) fusion(bf16[4096,16]{0,1:T(8,128)(2,1)S(1)} %copy-done.6, s32[]{:T(128)S(6)} %select_n.52, bf16[2,384,4096]{2,1,0:T(8,128)(2,1)} %param.10, f32[2,384]{1,0:T(2,128)S(1)} %add_rsqrt_fusion, f32[2,4,384]{2,1,0:T(4,128)S(1)} %reduce_window_sum.16, f32[2,4]{1,0:T(2,128)S(1)} %add.123), kind=kOutput, calls=%fused_computation.73 | convolution fusion | flops 34612216 | bytes 6352932 | tf_op jit(solution)/shard_map/spd,dh->sph/dot_general | solution.py:50
  46.5 17.1 %pmax.7 = f32[2,4]{1,0:T(2,128)S(1)} all-reduce(f32[2,4]{1,0:T(2,128)S(1)} %get-tuple-element.143), channel_id=1, replica_groups=mesh['sp'=8,'tp'=4] {'sp'}, use_global_device_ids=true, to_apply=%region_6.7 | all-reduce | flops 8 | bytes 64 | tf_op jit(solution)/shard_map/pmax | solution.py:59
  63.6 0.0 copy-start.4
  63.6 7.5 %fusion.27 = bf16[2,48,4,8,128]{4,3,2,1,0:T(8,128)(2,1)S(1)} fusion(bf16[4096,512]{1,0:T(8,128)(2,1)} %param.11, bf16[2,384,4096]{2,1,0:T(8,128)(2,1)} %param.10, f32[2,384]{1,0:T(2,128)S(1)} %add_rsqrt_fusion), kind=kOutput, calls=%fused_computation.15 | convolution fusion | flops 3231055872 | bytes 11275264 | tf_op jit(solution)/shard_map/spd,dc->spc/dot_general | solution.py:44
  71.1 0.0 copy-start.1
  71.1 0.1 fusion.98
  71.2 0.8 copy-done.1
  72.0 0.2 fusion.48
  72.2 0.2 copy.32
  72.4 0.7 reshape.95
  73.1 0.0 reduce-scatter.7.cloned.1.call-update
  73.2 0.0 reduce-scatter.5.cloned.1.call-start
  73.2 0.1 subtract_exponential_fusion
  73.3 6.9 %fusion.17 = f32[2,384,512]{2,1,0:T(8,128)S(1)} fusion(bf16[4096,512]{1,0:T(8,128)(2,1)} %param.12, bf16[2,384,4096]{2,1,0:T(8,128)(2,1)} %param.10, f32[2,384]{1,0:T(2,128)S(1)} %add_rsqrt_fusion), kind=kOutput, calls=%fused_computation.13 | convolution fusion | flops 3231449088 | bytes 12061696 | tf_op jit(solution)/shard_map/spd,dc->spc/dot_general | solution.py:47
  80.2 0.0 copy-start.5
  80.2 0.5 copy.31
  80.7 2.3 %fusion.47 = f32[2,4,128,128]{3,2,1,0:T(8,128)} fusion(f32[2,384,4,128]{1,3,2,0:T(8,128)S(1)} %bitcast.62, f32[2,384,4]{1,2,0:T(4,128)S(1)} %subtract_exponential_fusion, bf16[2,48,4,8,128]{4,3,2,1,0:T(8,128)(2,1)} %copy-done.1), kind=kOutput, calls=%fused_computation.27 | convolution fusion | flops 101449728 | bytes 2895872 | tf_op jit(solution)/shard_map/sthe,sthd->shed/dot_general | solution.py:65
  83.0 0.0 reduce-scatter.5.cloned.1.call-update
  83.0 0.0 copy-done.5
  83.0 5.2 %all_gather.13 = bf16[2,4096]{1,0:T(2,128)(2,1)S(1)} all-gather(bf16[2,1024]{1,0:T(2,128)(2,1)S(1)} %copy-done.5), channel_id=1, replica_groups=mesh['sp'=8,'tp'=4] {'tp'}, dimensions={1}, use_global_device_ids=true | all-gather | bytes 20480 | tf_op jit(solution)/shard_map/all_gather | solution.py:73
  88.2 0.1 fusion.54
  88.4 2.9 %fusion.44 = f32[2,512]{1,0:T(2,128)S(1)} fusion(bf16[4096,512]{1,0:T(8,128)(2,1)} %param.12, bf16[2,4096]{1,0:T(2,128)(2,1)S(1)} %all_gather.13, f32[2]{0:T(128)S(1)} %add_rsqrt_fusion.1), kind=kOutput, calls=%fused_computation.21 | convolution fusion | flops 8415232 | bytes 4214792 | tf_op jit(solution)/shard_map/dot_general | solution.py:78
  91.3 2.9 %convolution_convert_fusion.2 = bf16[2,512]{1,0:T(2,128)(2,1)S(1)} fusion(bf16[4096,512]{1,0:T(8,128)(2,1)} %param.13, bf16[2,4096]{1,0:T(2,128)(2,1)S(1)} %all_gather.13, f32[2]{0:T(128)S(1)} %add_rsqrt_fusion.1), kind=kOutput, calls=%fused_computation.24 | convolution fusion | flops 8414208 | bytes 4212744 | tf_op jit(solution)/shard_map/dot_general | solution.py:74
  94.2 2.9 %fusion.45 = f32[2,512]{1,0:T(2,128)S(1)} fusion(bf16[4096,512]{1,0:T(8,128)(2,1)} %param.11, bf16[2,4096]{1,0:T(2,128)(2,1)S(1)} %all_gather.13, f32[2]{0:T(128)S(1)} %add_rsqrt_fusion.1), kind=kOutput, calls=%fused_computation.23 | convolution fusion | flops 8415232 | bytes 4214792 | tf_op jit(solution)/shard_map/dot_general | solution.py:77
  97.1 0.1 multiply_reduce_fusion.1
  97.2 0.2 fusion.58
  97.4 37.1 %reduce-scatter.7.cloned.1.call-done = f32[16,8]{1,0:T(8,128)} async-done(((f32[128,8]{1,0:T(8,128)}), f32[16,8]{1,0:T(8,128)}) %reduce-scatter.7.cloned.1.call-update) | async-done | bytes 528
  134.6 0.8 reshape.96
  135.3 0.1 copy.33
  135.4 0.0 copy-start.3
  135.4 0.2 multiply_reduce_fusion
  135.6 18.6 %all-gather.2 = f32[8,2,4]{2,1,0:T(2,128)S(1)} all-gather(f32[1,2,4]{2,1,0:T(2,128)S(1)} %bitcast.69), channel_id=3, replica_groups=mesh['sp'=8,'tp'=4] {'sp'}, dimensions={0}, use_global_device_ids=true | all-gather | bytes 288 | tf_op jit(solution)/shard_map/all_gather | solution.py:100
  154.2 0.0 copy-done.4
  154.2 0.2 abs_maximum_fusion
  154.5 45.2 %reduce-scatter.5.cloned.1.call-done = f32[2,4,16,128]{3,2,1,0:T(8,128)} async-done(((f32[2,4,128,128]{3,2,1,0:T(8,128)}), f32[2,4,16,128]{3,2,1,0:T(8,128)}) %reduce-scatter.5.cloned.1.call-update) | async-done | bytes 65552 | tf_op jit(solution)/shard_map/reduce_scatter | solution.py:69
  199.6 0.8 convert_element_type.54
  200.5 0.0 copy-start.2
  200.5 0.1 fusion.92
  200.6 0.7 fusion.70
  201.3 0.0 copy-done.3
  201.3 0.0 copy-done.2
  (22 shorter events, 0.3 us)
Async XLA Ops:
  7.2 4.3 %copy-start = (bf16[4096,16]{0,1:T(8,128)(2,1)S(1)}, bf16[4096,16]{0,1:T(8,128)(2,1)}, u32[]{:S(2)}) copy-start(bf16[4096,16]{0,1:T(8,128)(2,1)} %param.15) | copy-start | bytes 393220
  7.2 4.2 %copy-start.7 = (f32[16]{0:T(128)S(1)}, f32[16]{0:T(128)}, u32[]{:S(2)}) copy-start(f32[16]{0:T(128)} %param.16) | copy-start | bytes 196
  7.2 127.4 %reduce-scatter.7.cloned.1.call-start = ((), (), s32[]{:S(2)}) async-start(), calls=%async_computation.3 | async-start | bytes 73728
  7.2 34.6 %copy-start.6 = (bf16[4096,16]{0,1:T(8,128)(2,1)S(1)}, bf16[4096,16]{0,1:T(8,128)(2,1)}, u32[]{:S(2)}) copy-start(bf16[4096,16]{0,1:T(8,128)(2,1)} %param.14) | copy-start | bytes 393220
  63.6 90.6 %copy-start.4 = (f32[2,4]{1,0:T(2,128)}, f32[2,4]{1,0:T(2,128)S(1)}, u32[]{:S(2)}) copy-start(f32[2,4]{1,0:T(2,128)S(1)} %pmax.7) | copy-start | bytes 100
  71.1 0.9 copy-start.1
  73.2 126.5 %reduce-scatter.5.cloned.1.call-start = ((), (), s32[]{:S(2)}) async-start(), calls=%async_computation.2 | async-start | bytes 589824 | tf_op jit(solution)/shard_map/reduce_scatter | solution.py:69
  80.2 2.8 %copy-start.5 = (bf16[2,1024]{1,0:T(2,128)(2,1)S(1)}, bf16[2,1024]{1,0:T(2,128)(2,1)}, u32[]{:S(2)}) copy-start(bf16[2,1024]{1,0:T(2,128)(2,1)} %param.17) | copy-start | bytes 12292
  135.4 65.8 %copy-start.3 = (f32[2,4,16]{2,1,0:T(4,128)}, f32[2,4,16]{2,1,0:T(4,128)S(1)}, u32[]{:S(2)}) copy-start(f32[2,4,16]{2,1,0:T(4,128)S(1)} %copy.33) | copy-start | bytes 1540
  200.5 0.8 copy-start.2
Sparse Core Ops, SparseCore 0:
  73.3 61.2 reduce-scatter.6
  137.9 61.6 reduce-scatter.4
